TPU v7x, 32 devices: a whole 2x2x4 slice. The times are simulated.
32 devices in a mesh: kv: 16 (over z, y, x), tp: 2 (over core).
Axes of the slice: x: 2, y: 2, z: 4, core: 2. Of those that a mesh axis runs over, the one named last changes fastest.
Arguments:
- tokens: bfloat16 [4096, 2048], P('kv'), may hold values from -72 to 72
- w_query: bfloat16 [2048, 1024], P(None, 'tp'), may hold values from -0.125 to 0.125
- w_key: bfloat16 [2048, 1024], P(None, 'tp'), may hold values from -0.125 to 0.125
- w_value: bfloat16 [2048, 1024], P(None, 'tp'), may hold values from -0.125 to 0.125
- w_out: bfloat16 [1024, 2048], P('tp'), may hold values from -0.1875 to 0.1875
- chosen: int32 [64, 16], replicated, may hold values from -1 to 63, as said below
Outputs:
- mixed: bfloat16 [4096, 2048], P(('kv', 'tp'))
- log_sums: float32 [16, 4096], P('tp', 'kv')
Inputs may be any that keep to these rules, and one draw needn't show every extreme that they name: `chosen`: row b begins with b itself, then lists distinct key blocks at most b, then holds -1 in its remaining entries. Taken together, the rows of the query blocks of one index of kv list at most 2 distinct blocks of the positions of any other index of kv, and exactly 2 for some pairs of indices in every draw.
All inputs are finite; a program needn't handle non-finite values.
Results may differ from a plain program's by a relative error of at most 0.03.
Values may be sent and summed in bfloat16 or wider, within the bound.
A program may use at most 64 MiB of HBM per device.

v0:
```python
import jax
import jax.numpy as jnp
from jax import lax
from jax.sharding import PartitionSpec as P

HEAD_DIM = 64
BLK = 64
SEL = 16
CAP = 2


rotary_base = 500000.0
masked_score = -1e30


def rotate(values, positions, head_count, head_size):
    half_size = head_size // 2
    inverse = rotary_base ** (-jnp.arange(half_size, dtype=jnp.float32) / half_size)
    angles = positions.astype(jnp.float32)[:, None, None] * inverse[None, None, :]
    cos_part = jnp.cos(angles)
    sin_part = jnp.sin(angles)
    grouped = values.reshape(values.shape[0], head_count, head_size)
    first_half = grouped[..., :half_size]
    second_half = grouped[..., half_size:]
    turned = jnp.concatenate(
        [
            first_half * cos_part - second_half * sin_part,
            second_half * cos_part + first_half * sin_part,
        ],
        axis=-1,
    )
    return turned.reshape(values.shape)


def local(tokens, w_query, w_key, w_value, w_out, chosen):
    local_rows = tokens.shape[0]
    local_width = w_query.shape[1]
    head_count = local_width // HEAD_DIM
    scaling = HEAD_DIM ** (-0.5)
    device = lax.axis_index("kv")
    positions = device * local_rows + jnp.arange(local_rows)
    query = rotate(
        jnp.dot(tokens, w_query, preferred_element_type=jnp.float32),
        positions,
        head_count,
        HEAD_DIM,
    ).astype(jnp.bfloat16)
    keys_here = rotate(
        jnp.dot(tokens, w_key, preferred_element_type=jnp.float32), positions, head_count, HEAD_DIM
    ).astype(jnp.bfloat16)
    values_here = jnp.dot(tokens, w_value, preferred_element_type=jnp.float32).astype(jnp.bfloat16)
    blocks_here = local_rows // BLK
    own_lists = lax.dynamic_slice_in_dim(chosen, device * blocks_here, blocks_here, 0)
    query_heads = query.reshape(local_rows, head_count, HEAD_DIM)
    devices = lax.axis_size("kv")
    mine_blocks = device * blocks_here + jnp.arange(blocks_here)
    listed_hits = jnp.any(chosen[:, :, None] == mine_blocks[None, None, :], axis=1)
    wanted = jnp.any(listed_hits.reshape(devices, blocks_here, blocks_here), axis=1)
    wanted = wanted & (jnp.arange(devices) != device)[:, None]
    send_slots = jnp.cumsum(wanted.astype(jnp.int32), axis=1) - 1
    placing = (wanted[:, None, :] & (send_slots[:, None, :] == jnp.arange(CAP)[:, None])).astype(
        jnp.bfloat16
    )
    both_here = jnp.concatenate([keys_here, values_here], axis=1).reshape(
        blocks_here, BLK, 2 * local_width
    )
    outgoing = (
        jnp.einsum("dcb,bkf->dckf", placing, both_here, preferred_element_type=jnp.float32)
        .astype(jnp.bfloat16)
        .reshape(devices, CAP * BLK, 2 * local_width)
    )
    incoming = lax.all_to_all(outgoing, "kv", split_axis=0, concat_axis=0, tiled=True)
    every_block = jnp.arange(chosen.shape[0])
    needed = jnp.any(own_lists.reshape(-1)[:, None] == every_block[None, :], axis=0).reshape(
        devices, blocks_here
    )
    my_slots = (jnp.cumsum(needed.astype(jnp.int32), axis=1) - 1).reshape(-1)
    usable = own_lists >= 0
    safe_rows = jnp.maximum(own_lists, 0)
    lookup = jnp.sum(
        jnp.where(safe_rows[:, :, None] == every_block[None, None, :], my_slots[None, None, :], 0),
        axis=-1,
    )
    owner_dev = safe_rows // blocks_here
    source_row = jnp.where(
        owner_dev == device, devices * CAP + safe_rows % blocks_here, owner_dev * CAP + lookup
    )
    key_table = jnp.concatenate(
        [incoming.reshape(devices * CAP, BLK, 2 * local_width), both_here], axis=0
    )
    picked = key_table[source_row]
    picked_keys = picked[..., :local_width].reshape(blocks_here, SEL * BLK, head_count, HEAD_DIM)
    picked_values = picked[..., local_width:].reshape(blocks_here, SEL * BLK, head_count, HEAD_DIM)
    query_blocks = query_heads.reshape(blocks_here, BLK, head_count, HEAD_DIM)
    scores = (
        jnp.einsum("bqhd,bkhd->bhqk", query_blocks, picked_keys, preferred_element_type=jnp.float32)
        * scaling
    )
    key_mask = jnp.broadcast_to(usable[:, :, None], (blocks_here, SEL, BLK)).reshape(
        blocks_here, 1, 1, SEL * BLK
    )
    scores = jnp.where(key_mask, scores, masked_score)
    block_max = jnp.max(scores, axis=-1)
    weights = jnp.where(key_mask, jnp.exp(scores - block_max[..., None]), 0.0)
    block_total = jnp.sum(weights, axis=-1)
    block_sum = jnp.einsum(
        "bhqk,bkhd->bhqd",
        weights.astype(jnp.bfloat16),
        picked_values,
        preferred_element_type=jnp.float32,
    )
    row_max = jnp.transpose(block_max, (1, 0, 2)).reshape(head_count, local_rows)
    totals = jnp.transpose(block_total, (1, 0, 2)).reshape(head_count, local_rows)
    summed = jnp.transpose(block_sum, (1, 0, 2, 3)).reshape(head_count, local_rows, HEAD_DIM)
    mixed_heads = summed / totals[..., None]
    attended = (
        jnp.transpose(mixed_heads, (1, 0, 2)).reshape(local_rows, local_width).astype(jnp.bfloat16)
    )
    log_sums = row_max + jnp.log(totals)
    output = lax.psum_scatter(
        jnp.dot(attended, w_out, preferred_element_type=jnp.float32).astype(jnp.bfloat16),
        "tp",
        scatter_dimension=0,
        tiled=True,
    )
    return (output, log_sums)


def solution(mesh):
    placed = (P("kv", None), P(None, "tp"), P(None, "tp"), P(None, "tp"), P("tp", None), P())
    return jax.shard_map(
        local,
        mesh=mesh,
        in_specs=placed,
        out_specs=(P(("kv", "tp"), None), P("tp", "kv")),
        check_vma=False,
    )
```

profile of v0, /device:TPU:25, one launch (start us, length us, event | category | flops | bytes accessed | tf_op | source)
XLA Modules:
  0.0 209.6 jit_solution(15271274122872294432)
XLA Ops:
  7.2 0.9 compare_reduce_fusion
  8.5 2.6 %convolution_convert_fusion.2 = bf16[256,512]{1,0:T(8,128)(2,1)S(1)} fusion(bf16[256,2048]{1,0:T(8,128)(2,1)} %param.6, bf16[2048,512]{1,0:T(8,128)(2,1)} %param.9), kind=kOutput, calls=%fused_computation.19 | convolution fusion | flops 537001984 | bytes 3407872 | tf_op jit(solution)/shard_map/dot_general | solution.py:51
  11.1 2.8 %fusion.35 = f32[256,512]{0,1:T(8,128)S(1)} fusion(bf16[256,2048]{1,0:T(8,128)(2,1)} %param.6, bf16[2048,512]{1,0:T(8,128)(2,1)} %param.7), kind=kOutput, calls=%fused_computation.67 | convolution fusion | flops 536870912 | bytes 3670016 | tf_op jit(solution)/shard_map/dot_general | solution.py:43
  14.0 2.8 %fusion.36 = f32[256,512]{0,1:T(8,128)S(1)} fusion(bf16[256,2048]{1,0:T(8,128)(2,1)} %param.6, bf16[2048,512]{1,0:T(8,128)(2,1)} %param.8), kind=kOutput, calls=%fused_computation.68 | convolution fusion | flops 536870912 | bytes 3670016 | tf_op jit(solution)/shard_map/dot_general | solution.py:49
  17.5 1.6 convolution_convert_fusion
  19.1 4.3 %copy.90 = bf16[16,128,1024]{2,1,0:T(8,128)(2,1)} copy(bf16[16,128,1024]{2,0,1:T(8,128)(2,1)S(1)} %bitcast.41) | data formatting | bytes 8388608 | tf_op jit(solution)/shard_map/reshape | solution.py:70
  23.4 6.4 %all-to-all-start = ((bf16[16,128,1024]{2,1,0:T(8,128)(2,1)}), bf16[16,128,1024]{2,1,0:T(8,128)(2,1)}, u32[]{:S(2)}, u32[]{:S(2)}) async-start(bf16[16,128,1024]{2,1,0:T(8,128)(2,1)} %copy.90), calls=%async_computation | async-start | bytes 8388608 | tf_op jit(solution)/shard_map/all_to_all | solution.py:72
  31.2 0.2 convert_element_type.53
  31.4 85.9 %all-to-all-done = bf16[16,128,1024]{2,1,0:T(8,128)(2,1)} async-done(((bf16[16,128,1024]{2,1,0:T(8,128)(2,1)}), bf16[16,128,1024]{2,1,0:T(8,128)(2,1)}, u32[]{:S(2)}, u32[]{:S(2)}) %all-to-all-start) | async-done | bytes 4194336 | tf_op jit(solution)/shard_map/all_to_all | solution.py:72
  117.4 4.7 %pad_maximum_fusion = bf16[36,64,1024]{2,1,0:T(8,128)(2,1)} fusion(bf16[4,64,1024]{2,1,0:T(8,128)(2,1)S(1)} %bitcast.43, bf16[32,64,1024]{2,1,0:T(8,128)(2,1)} %bitcast.8), kind=kLoop, calls=%fused_computation.10 | loop fusion | flops 2359296 | bytes 9437184 | tf_op jit(solution)/shard_map/concatenate | solution.py:88
  122.1 8.0 %gather_fusion = bf16[64,64,1024]{2,1,0:T(8,128)(2,1)} fusion(bf16[36,64,1024]{2,1,0:T(8,128)(2,1)} %pad_maximum_fusion, s32[1024]{0:T(1024)S(1)} %pad_clamp_fusion), kind=kCustom, calls=%fused_computation | custom fusion | bytes 16777472 | tf_op jit(solution)/shard_map/gather | solution.py:91
  130.1 5.9 %fusion.34 = (bf16[4,16,64,512]{3,2,1,0:T(8,128)(2,1)}, bf16[4,16,64,512]{3,2,1,0:T(8,128)(2,1)}) fusion(bf16[4,16,64,1024]{3,2,1,0:T(8,128)(2,1)} %bitcast.40), kind=kLoop, calls=%fused_computation.66 | loop fusion | bytes 16777216 | tf_op jit(solution)/shard_map/slice | solution.py:92
  136.0 11.2 %reshape.176 = bf16[4,1024,8,64]{3,2,1,0:T(8,128)(2,1)} reshape(bf16[4,16,64,512]{3,2,1,0:T(8,128)(2,1)} %get-tuple-element.4) | data formatting | bytes 8388608 | tf_op jit(solution)/shard_map/reshape | solution.py:92
  147.2 6.5 %fusion.4 = (f32[4,8,64]{2,1,0:T(8,128)S(1)}, f32[4,8,64,1024]{3,2,1,0:T(8,128)S(1)}) fusion(pred[4,1024]{1,0:T(4,128)(4,1)S(1)} %broadcast_in_dim.55, bf16[4,1024,8,64]{3,2,1,0:T(8,128)(2,1)} %reshape.176, bf16[4,64,8,64]{1,0,3,2:T(4,128)(2,1)S(1)} %convert_element_type.53), kind=kOutput, calls=%fused_computation.7 | convolution fusion | flops 274724864 | bytes 12857344 | tf_op jit(solution)/shard_map/bqhd,bkhd->bhqk/dot_general | solution.py:96
  153.7 3.2 %copy-done.1 = f32[4,8,64,1024]{3,2,1,0:T(8,128)} copy-done((f32[4,8,64,1024]{3,2,1,0:T(8,128)}, f32[4,8,64,1024]{3,2,1,0:T(8,128)S(1)}, u32[]{:S(2)}) %copy-start.1) | copy-done | bytes 8388632
  156.9 2.3 %fusion.5 = f32[4,8,64]{2,1,0:T(8,128)S(1)} fusion(f32[4,8,64,1024]{3,2,1,0:T(8,128)S(1)} %get-tuple-element.15, f32[4,8,64]{2,1,0:T(8,128)S(1)} %get-tuple-element.14, pred[4,1024]{1,0:T(4,128)(4,1)S(1)} %broadcast_in_dim.55), kind=kLoop, calls=%fused_computation.8 | loop fusion | flops 10483712 | bytes 8409088 | tf_op jit(solution)/shard_map/reduce_sum | solution.py:105
  159.2 11.2 %reshape.177 = bf16[4,1024,8,64]{3,2,1,0:T(8,128)(2,1)} reshape(bf16[4,16,64,512]{3,2,1,0:T(8,128)(2,1)} %get-tuple-element.5) | data formatting | bytes 8388608 | tf_op jit(solution)/shard_map/reshape | solution.py:93
  170.4 10.2 %fusion.13 = f32[8,4,64,64]{3,2,0,1:T(8,128)} fusion(bf16[4,1024,8,64]{3,2,1,0:T(8,128)(2,1)} %reshape.177, f32[4,8,64,1024]{3,2,1,0:T(8,128)} %copy-done.1, f32[4,8,64]{2,1,0:T(8,128)S(1)} %get-tuple-element.14, pred[4,1024]{1,0:T(4,128)(4,1)S(1)} %broadcast_in_dim.55), kind=kOutput, calls=%fused_computation.18 | convolution fusion | flops 278921216 | bytes 13119488 | tf_op jit(solution)/shard_map/bhqk,bkhd->bhqd/dot_general | solution.py:106
  180.6 1.6 copy.96
  182.2 1.4 reshape.178
  183.6 1.1 divide_convert_fusion
  184.7 1.7 convolution_convert_fusion.1
  186.6 0.6 log_add_fusion
  187.2 15.5 %reduce-scatter.2.cloned.1.call-done = bf16[128,2048]{1,0:T(8,128)(2,1)} async-done(((bf16[256,2048]{1,0:T(8,128)(2,1)}), bf16[128,2048]{1,0:T(8,128)(2,1)}) %reduce-scatter.2.cloned.1.call-update) | async-done | bytes 524304 | tf_op jit(solution)/shard_map/reduce_scatter | solution.py:120
  (44 shorter events, 2.4 us)
Async XLA Ops:
  7.2 177.6 %copy-start = (bf16[512,2048]{1,0:T(8,128)(2,1)S(1)}, bf16[512,2048]{1,0:T(8,128)(2,1)}, u32[]{:S(2)}) copy-start(bf16[512,2048]{1,0:T(8,128)(2,1)} %param.10) | copy-start | bytes 6291460
  19.1 10.8 %copy-start.2 = (s32[64,16]{0,1:T(8,128)S(1)}, s32[64,16]{0,1:T(8,128)}, u32[]{:S(2)}) copy-start(s32[64,16]{0,1:T(8,128)} %param.11) | copy-start | bytes 12292
  23.4 93.9 %all-to-all-start = ((bf16[16,128,1024]{2,1,0:T(8,128)(2,1)}), bf16[16,128,1024]{2,1,0:T(8,128)(2,1)}, u32[]{:S(2)}, u32[]{:S(2)}) async-start(bf16[16,128,1024]{2,1,0:T(8,128)(2,1)} %copy.90), calls=%async_computation | async-start | bytes 8388608 | tf_op jit(solution)/shard_map/all_to_all | solution.py:72
  29.8 172.9 %reduce-scatter.2.cloned.1.call-start = ((), (), s32[]{:S(2)}) async-start(), calls=%async_computation.2 | async-start | bytes 1572864 | tf_op jit(solution)/shard_map/reduce_scatter | solution.py:120
  153.7 3.2 %copy-start.1 = (f32[4,8,64,1024]{3,2,1,0:T(8,128)}, f32[4,8,64,1024]{3,2,1,0:T(8,128)S(1)}, u32[]{:S(2)}) copy-start(f32[4,8,64,1024]{3,2,1,0:T(8,128)S(1)} %get-tuple-element.15) | copy-start | bytes 25165828
Sparse Core Ops, SparseCore 0:
  186.6 16.0 reduce-scatter.1
where the time goes:
time: 211 us; the launch traced here: 210 us
  waiting for transfers between devices  101 us (48%)
  local copies, waits for them, and re-layouts  48.3 us (23%)
  matrix products  28.4 us (13%)
  between operations  14.3 us (7%)
  other arithmetic  10.7 us (5%)
  starting transfers between devices  6.48 us (3%)
    all_to_all x1, waiting for transfers between devices, local(): lax.all_to_all(outgoing, 'kv', split_axis=0, concat_axis=0, tiled=True)  85.9 us
    reduce_scatter x1, waiting for transfers between devices, local(): lax.psum_scatter(jnp.dot(attended, w_out, preferred_element_type=jnp.floa...  15.5 us
    reshape x1, local copies, waits for them, and re-layouts, local(): picked[..., local_width:]  11.2 us
    reshape x1, local copies, waits for them, and re-layouts, local(): picked[..., :local_width]  11.2 us
    dot_general x1, matrix products, local(): jnp.einsum('bhqk,bkhd->bhqd', weights.astype(jnp.bfloat16), picked_values...  10.2 us
    gather x1, local copies, waits for them, and re-layouts, local(): picked = key_table[source_row]  7.97 us
    dot_general x1, matrix products, local(): jnp.einsum('bqhd,bkhd->bhqk', query_blocks, picked_keys, preferred_elemen...  6.5 us
    all_to_all x1, starting transfers between devices, local(): lax.all_to_all(outgoing, 'kv', split_axis=0, concat_axis=0, tiled=True)  6.44 us
  transfers between devices with their start and end apart: 2, of which 2 were waited for; matrix products, arithmetic and copies ran while one was open for 1% of the time, Pallas kernels for 0%

commit v1 on v0

v1 whole, which is shorter than its diff:
```python
import functools

import jax
import jax.numpy as jnp
from jax import lax
from jax.experimental import pallas as pl
from jax.experimental.pallas import tpu as pltpu
from jax.sharding import PartitionSpec as P

HEAD_DIM = 64
BLK = 64
CAP = 2
LANES = 128
VMEM_LIMIT = 48 * 1024 * 1024

rotary_base = 500000.0
masked_score = -1e30


def in_vmem():
    return pl.BlockSpec(memory_space=pltpu.VMEM)


def in_smem():
    return pl.BlockSpec(memory_space=pltpu.SMEM)


def project_kernel(tiles, x_ref, wk_ref, wv_ref, wq_ref, cos_ref, sin_ref, kv_ref, q_ref):
    step = pl.program_id(0)
    half = HEAD_DIM // 2
    cos_part = cos_ref[...]
    sin_part = sin_ref[...]
    low = lax.broadcasted_iota(jnp.int32, cos_part.shape, 1) % HEAD_DIM < half

    def turned(values):
        parts = []
        for lane in range(0, values.shape[1], LANES):
            part = values[:, lane : lane + LANES]
            other = jnp.where(low, pltpu.roll(part, LANES - half, 1), pltpu.roll(part, half, 1))
            parts.append(part * cos_part + other * sin_part)
        return jnp.concatenate(parts, axis=1) if len(parts) > 1 else parts[0]

    @pl.when(step < tiles)
    def _():
        made = jnp.dot(x_ref[...], wk_ref[...], preferred_element_type=jnp.float32)
        kv_ref[0] = turned(made).astype(jnp.bfloat16)

    @pl.when((step >= tiles) & (step < 2 * tiles))
    def _():
        made = jnp.dot(x_ref[...], wv_ref[...], preferred_element_type=jnp.float32)
        kv_ref[0] = made.astype(jnp.bfloat16)

    @pl.when(step >= 2 * tiles)
    def _():
        made = jnp.dot(x_ref[...], wq_ref[...], preferred_element_type=jnp.float32)
        q_ref[...] = (turned(made).astype(jnp.bfloat16) * (HEAD_DIM**-0.5)).astype(jnp.bfloat16)


def exchange_kernel(
    layers, group, blocks, sel_ref, kv_ref, tab_ref, stage, col_send, col_recv, pl_send, pl_recv, own_sem
):
    chunks = kv_ref.shape[0]
    me = lax.axis_index("kv")
    z = lax.div(me, group)
    g = lax.rem(me, group)
    up = lax.rem(me + group, layers * group)
    down = lax.rem(me + (layers - 1) * group, layers * group)
    span = blocks * BLK

    barrier = pltpu.get_barrier_semaphore()
    peers = [z * group + lax.rem(g + d, group) for d in range(group)]
    for d in range(1, group):
        pl.semaphore_signal(barrier, inc=1, device_id={"kv": peers[d]}, device_id_type=pl.DeviceIdType.MESH)

    @pl.when(z < layers - 1)
    def _():
        pl.semaphore_signal(barrier, inc=1, device_id={"kv": up}, device_id_type=pl.DeviceIdType.MESH)

    @pl.when(z > 0)
    def _():
        pl.semaphore_signal(barrier, inc=1, device_id={"kv": down}, device_id_type=pl.DeviceIdType.MESH)

    pl.semaphore_wait(barrier, group - 1 + jnp.minimum(z, 1) + jnp.minimum(layers - 1 - z, 1))

    own = pltpu.make_async_copy(kv_ref, tab_ref.at[:, pl.ds(0, span)], own_sem)
    own.start()

    def column(t, ch):
        return tab_ref.at[ch, pl.ds(t * span, span)]

    def column_copy(t, ch):
        source = kv_ref.at[ch] if t == 0 else column(t, ch)
        return pltpu.make_async_remote_copy(
            src_ref=source,
            dst_ref=column(t + 1, ch),
            send_sem=col_send.at[t, ch],
            recv_sem=col_recv.at[t, ch],
            device_id={"kv": up},
            device_id_type=pl.DeviceIdType.MESH,
        )

    def plane_copy(d, t, ch):
        place = (layers * blocks + ((d - 1) * layers + t) * CAP) * BLK
        return pltpu.make_async_remote_copy(
            src_ref=stage.at[d - 1, t, ch],
            dst_ref=tab_ref.at[ch, pl.ds(place, CAP * BLK)],
            send_sem=pl_send.at[d - 1, t, ch],
            recv_sem=pl_recv.at[d - 1, t, ch],
            device_id={"kv": peers[d]},
            device_id_type=pl.DeviceIdType.MESH,
        )

    for t in range(layers):

        @pl.when(z >= t)
        def _():
            def one_chunk(ch, carry):
                if t > 0:
                    column_copy(t - 1, ch).wait_recv()
                if t < layers - 1:

                    @pl.when(z < layers - 1)
                    def _():
                        column_copy(t, ch).start()

                def hand_on(d):
                    for c in range(CAP):
                        index = sel_ref[peers[d], ((z - t) * group + g) * CAP + c]
                        picked = None
                        for i in range(blocks):
                            source = kv_ref if t == 0 else tab_ref
                            tile = source[ch, pl.ds(t * span + i * BLK, BLK), :]
                            picked = tile if picked is None else jnp.where(index == i, tile, picked)
                        stage[d - 1, t, ch, pl.ds(c * BLK, BLK), :] = picked
                    plane_copy(d, t, ch).start()

                for d in range(1, group):
                    if t == 0:
                        pl.when(g + d < group)(functools.partial(hand_on, d))
                    else:
                        hand_on(d)
                return carry

            lax.fori_loop(0, chunks, one_chunk, 0)

    own.wait()
    for t in range(layers):

        @pl.when(z >= t)
        def _():
            def one_chunk(ch, carry):
                if t < layers - 1:

                    @pl.when(z < layers - 1)
                    def _():
                        column_copy(t, ch).wait_send()

                for d in range(1, group):
                    if t == 0:
                        pl.when(g + d < group)(lambda d=d: plane_copy(d, t, ch).wait_send())
                        pl.when(g >= d)(lambda d=d: plane_copy(d, t, ch).wait_recv())
                    else:
                        plane_copy(d, t, ch).wait_send()
                        plane_copy(d, t, ch).wait_recv()
                return carry

            lax.fori_loop(0, chunks, one_chunk, 0)


def attend_kernel(
    layers, group, blocks, chosen_ref, slot_ref, q_ref, tab_ref, out_ref, log_ref, keys, values
):
    chunks = tab_ref.shape[0]
    wide = tab_ref.shape[2]
    entries = chosen_ref.shape[1]
    width = q_ref.shape[1]
    me = lax.axis_index("kv")
    z = lax.div(me, group)
    g = lax.rem(me, group)

    def one_block(r, carry):
        mine = me * blocks + r
        count = 0
        for s in range(entries):
            listed = chosen_ref[mine, s]
            count = count + jnp.where(listed >= 0, 1, 0)
            block = jnp.where(listed >= 0, listed, mine)
            owner = lax.div(block, blocks)
            t = z - lax.div(owner, group)
            d = lax.rem(g - lax.rem(owner, group) + group, group)
            row = jnp.where(
                d == 0,
                t * blocks + lax.rem(block, blocks),
                layers * blocks + ((d - 1) * layers + t) * CAP + slot_ref[me, block],
            )
            start = pl.multiple_of(row * BLK, BLK)
            for ch in range(chunks // 2):
                lanes = slice(ch * wide, (ch + 1) * wide)
                keys[s * BLK : (s + 1) * BLK, lanes] = tab_ref[ch, pl.ds(start, BLK), :]
                values[s * BLK : (s + 1) * BLK, lanes] = tab_ref[chunks // 2 + ch, pl.ds(start, BLK), :]
        rows = pl.ds(pl.multiple_of(r * BLK, BLK), BLK)
        first = lax.broadcasted_iota(jnp.int32, (BLK, LANES), 1) < HEAD_DIM
        lane = lax.broadcasted_iota(jnp.int32, (BLK, LANES), 1)
        live = lax.broadcasted_iota(jnp.int32, (2 * BLK, entries * BLK), 1) < count * BLK
        logs = jnp.zeros((BLK, LANES), jnp.float32)
        for pair in range(width // LANES):
            lanes = slice(pair * LANES, (pair + 1) * LANES)
            both = q_ref[rows, lanes]
            none = jnp.zeros_like(both)
            stacked = jnp.concatenate([jnp.where(first, both, none), jnp.where(first, none, both)], axis=0)
            scores = lax.dot_general(
                stacked, keys[:, lanes], (((1,), (1,)), ((), ())), preferred_element_type=jnp.float32
            )
            scores = jnp.where(live, scores, masked_score)
            top = jnp.max(scores, axis=1, keepdims=True)
            weights = jnp.exp(scores - top)
            total = jnp.sum(weights, axis=1, keepdims=True)
            summed = jnp.dot(
                weights.astype(jnp.bfloat16), values[:, lanes], preferred_element_type=jnp.float32
            )
            summed = summed / total
            out_ref[rows, lanes] = jnp.where(first, summed[:BLK], summed[BLK:]).astype(jnp.bfloat16)
            log_sum = top + jnp.log(total)
            logs = jnp.where(lane == 2 * pair, log_sum[:BLK], logs)
            logs = jnp.where(lane == 2 * pair + 1, log_sum[BLK:], logs)
        log_ref[rows, :] = logs
        return carry

    lax.fori_loop(0, blocks, one_block, 0)


def mix_kernel(n, att_ref, w_ref, out_ref, stage, landed, send_sem, recv_sem):
    me = lax.axis_index("tp")
    rows = out_ref.shape[0]
    tile = min(512, w_ref.shape[1])
    tiles = w_ref.shape[1] // tile
    peers = [lax.rem(me + d, n) for d in range(n)]
    barrier = pltpu.get_barrier_semaphore()
    for d in range(1, n):
        pl.semaphore_signal(barrier, inc=1, device_id={"tp": peers[d]}, device_id_type=pl.DeviceIdType.MESH)
    pl.semaphore_wait(barrier, n - 1)

    def partial_of(d, j):
        mine = att_ref[pl.ds(pl.multiple_of(peers[d] * rows, rows), rows), :]
        made = jnp.dot(mine, w_ref[:, j * tile : (j + 1) * tile], preferred_element_type=jnp.float32)
        return made.astype(jnp.bfloat16)

    def hop(d, j):
        return pltpu.make_async_remote_copy(
            src_ref=stage.at[d - 1, j],
            dst_ref=landed.at[d - 1, j],
            send_sem=send_sem.at[d - 1, j],
            recv_sem=recv_sem.at[d - 1, j],
            device_id={"tp": peers[d]},
            device_id_type=pl.DeviceIdType.MESH,
        )

    for d in range(1, n):
        for j in range(tiles):
            stage[d - 1, j] = partial_of(d, j)
            hop(d, j).start()
    for j in range(tiles):
        acc = partial_of(0, j).astype(jnp.float32)
        for d in range(1, n):
            hop(d, j).wait_recv()
            acc = acc + landed[d - 1, j].astype(jnp.float32)
        out_ref[:, j * tile : (j + 1) * tile] = acc.astype(jnp.bfloat16)
    for d in range(1, n):
        for j in range(tiles):
            hop(d, j).wait_send()


def local(devices, splits, tokens, w_query, w_key, w_value, w_out, chosen):
    rows, depth = tokens.shape
    width = w_query.shape[1]
    heads = width // HEAD_DIM
    blocks = rows // BLK
    group = 1
    while group * group < devices:
        group *= 2
    layers = devices // group
    all_blocks = chosen.shape[0]
    me = lax.axis_index("kv")

    half = HEAD_DIM // 2
    inverse = rotary_base ** (-jnp.arange(half, dtype=jnp.float32) / half)
    positions = (me * rows + jnp.arange(rows)).astype(jnp.float32)
    angles = positions[:, None] * inverse[None, :]
    cos_half, sin_half = jnp.cos(angles), jnp.sin(angles)
    cos_part = jnp.concatenate([cos_half] * (LANES // half), axis=1)
    sin_part = jnp.concatenate([-sin_half, sin_half] * (LANES // HEAD_DIM), axis=1)

    wide = min(2 * LANES, width)
    tiles = width // wide
    chunks = 2 * tiles
    kv, query = pl.pallas_call(
        functools.partial(project_kernel, tiles),
        grid=(3 * tiles,),
        in_specs=[
            pl.BlockSpec((rows, depth), lambda j: (0, 0)),
            pl.BlockSpec((depth, wide), lambda j: (0, jnp.minimum(j, tiles - 1))),
            pl.BlockSpec((depth, wide), lambda j: (0, jnp.clip(j - tiles, 0, tiles - 1))),
            pl.BlockSpec((depth, wide), lambda j: (0, jnp.maximum(j - 2 * tiles, 0))),
            pl.BlockSpec((rows, LANES), lambda j: (0, 0)),
            pl.BlockSpec((rows, LANES), lambda j: (0, 0)),
        ],
        out_specs=[
            pl.BlockSpec((1, rows, wide), lambda j: (jnp.minimum(j, chunks - 1), 0, 0)),
            pl.BlockSpec((rows, wide), lambda j: (0, jnp.maximum(j - chunks, 0))),
        ],
        out_shape=[
            jax.ShapeDtypeStruct((chunks, rows, wide), jnp.bfloat16),
            jax.ShapeDtypeStruct((rows, width), jnp.bfloat16),
        ],
        compiler_params=pltpu.CompilerParams(
            dimension_semantics=("arbitrary",), vmem_limit_bytes=VMEM_LIMIT
        ),
        name="project",
    )(tokens, w_key, w_value, w_query, cos_part, sin_part)

    flat = chosen.reshape(devices, -1)
    listed = jnp.any(flat[:, :, None] == jnp.arange(all_blocks)[None, None, :], axis=1)
    listed = listed.reshape(devices, devices, blocks).astype(jnp.int32)
    before = (jnp.arange(blocks)[:, None] < jnp.arange(blocks)[None, :]).astype(jnp.int32)
    slots = jnp.sum(listed[:, :, :, None] * before[None, None], axis=2)
    fits = (slots[:, :, None, :] == jnp.arange(CAP)[:, None]) & (listed[:, :, None, :] > 0)
    sel = jnp.sum(jnp.where(fits, jnp.arange(blocks), 0), axis=-1).reshape(devices, devices * CAP)
    slots = jnp.minimum(slots, CAP - 1).reshape(devices, all_blocks)

    table_rows = (layers * blocks + (group - 1) * layers * CAP) * BLK
    table = pl.pallas_call(
        functools.partial(exchange_kernel, layers, group, blocks),
        in_specs=[in_smem(), in_vmem()],
        out_specs=in_vmem(),
        out_shape=jax.ShapeDtypeStruct((chunks, table_rows, wide), jnp.bfloat16),
        scratch_shapes=[
            pltpu.VMEM((group - 1, layers, chunks, CAP * BLK, wide), jnp.bfloat16),
            pltpu.SemaphoreType.DMA((layers, chunks)),
            pltpu.SemaphoreType.DMA((layers, chunks)),
            pltpu.SemaphoreType.DMA((group - 1, layers, chunks)),
            pltpu.SemaphoreType.DMA((group - 1, layers, chunks)),
            pltpu.SemaphoreType.DMA,
        ],
        compiler_params=pltpu.CompilerParams(
            collective_id=0, has_side_effects=True, vmem_limit_bytes=VMEM_LIMIT
        ),
        name="exchange",
    )(sel, kv)

    attended, logs = pl.pallas_call(
        functools.partial(attend_kernel, layers, group, blocks),
        in_specs=[in_smem(), in_smem(), in_vmem(), in_vmem()],
        out_specs=[in_vmem(), in_vmem()],
        out_shape=[
            jax.ShapeDtypeStruct((rows, width), jnp.bfloat16),
            jax.ShapeDtypeStruct((rows, LANES), jnp.float32),
        ],
        scratch_shapes=[pltpu.VMEM((chosen.shape[1] * BLK, width), jnp.bfloat16)] * 2,
        compiler_params=pltpu.CompilerParams(vmem_limit_bytes=VMEM_LIMIT),
        name="attend",
    )(chosen, slots, query, table)
    log_sums = jnp.transpose(logs[:, :heads])

    out_rows = rows // splits
    tile = min(512, w_out.shape[1])
    out_tiles = w_out.shape[1] // tile
    output = pl.pallas_call(
        functools.partial(mix_kernel, splits),
        in_specs=[in_vmem(), in_vmem()],
        out_specs=in_vmem(),
        out_shape=jax.ShapeDtypeStruct((out_rows, w_out.shape[1]), jnp.bfloat16),
        scratch_shapes=[
            pltpu.VMEM((splits - 1, out_tiles, out_rows, tile), jnp.bfloat16),
            pltpu.VMEM((splits - 1, out_tiles, out_rows, tile), jnp.bfloat16),
            pltpu.SemaphoreType.DMA((splits - 1, out_tiles)),
            pltpu.SemaphoreType.DMA((splits - 1, out_tiles)),
        ],
        compiler_params=pltpu.CompilerParams(
            collective_id=1, has_side_effects=True, vmem_limit_bytes=VMEM_LIMIT
        ),
        name="mix",
    )(attended, w_out)
    return (output, log_sums)


def solution(mesh):
    placed = (P("kv", None), P(None, "tp"), P(None, "tp"), P(None, "tp"), P("tp", None), P())
    return jax.shard_map(
        functools.partial(local, mesh.shape["kv"], mesh.shape["tp"]),
        mesh=mesh,
        in_specs=placed,
        out_specs=(P(("kv", "tp"), None), P("tp", "kv")),
        check_vma=False,
    )
```

time: 211 us -> 74.5 us (0.35)
  waiting for transfers between devices: 101 us -> 0 us
  Pallas kernels: 0 us -> 66.8 us
  local copies, waits for them, and re-layouts: 48.3 us -> 4.55 us
  matrix products: 28.4 us -> 0 us
  between operations: 14.3 us -> 0.78 us
  other arithmetic: 10.7 us -> 1.21 us
  starting transfers between devices: 6.48 us -> 0 us
    all_to_all x1 -> x0, waiting for transfers between devices: 85.9 us -> none  [local(): lax.all_to_all(outgoing, 'kv', split_axis=0, concat_axis=0, tiled=True)]
    pallas_call x0 -> x4, Pallas kernels: none -> 66.8 us  [the longest x1 49.4 us: local(): pl.pallas_call(functools.partial(exchange_kernel, layers, group, blocks),...]
    dot_general x7 -> x0, matrix products: 28.4 us -> none  [the longest x1 10.2 us: local(): jnp.einsum('bhqk,bkhd->bhqd', weights.astype(jnp.bfloat16), picked_values...]
    reshape x6 -> x1, local copies, waits for them, and re-layouts: 28.2 us -> 0.07 us  [local(): jnp.sum(jnp.where(fits, jnp.arange(blocks), 0), axis=-1)]
    reduce_scatter x1 -> x0, waiting for transfers between devices: 15.5 us -> none  [local(): lax.psum_scatter(jnp.dot(attended, w_out, preferred_element_type=jnp.floa...]
    gather x1 -> x0, local copies, waits for them, and re-layouts: 7.97 us -> none  [local(): picked = key_table[source_row]]
    all_to_all x1 -> x0, starting transfers between devices: 6.44 us -> none  [local(): lax.all_to_all(outgoing, 'kv', split_axis=0, concat_axis=0, tiled=True)]
    slice x1 -> x0, local copies, waits for them, and re-layouts: 5.94 us -> none  [local(): picked[..., :local_width]]
  transfers between devices with their start and end apart: 2 -> 0, of which waited for: 2 -> 0; matrix products, arithmetic and copies ran while one was open for 1% -> 0% of each run, Pallas kernels for 0% -> 0%
where the time goes in v1:
time: 74.5 us; the launch traced here: 73.3 us
  Pallas kernels  66.8 us (90%)
  local copies, waits for them, and re-layouts  4.55 us (6%)
  other arithmetic  1.21 us (2%)
  between operations  0.78 us (1%)
    pallas_call x1, Pallas kernels, local(): pl.pallas_call(functools.partial(exchange_kernel, layers, group, blocks),...  49.4 us
    pallas_call x1, Pallas kernels, local(): pl.pallas_call(functools.partial(attend_kernel, layers, group, blocks), i...  8.24 us
    pallas_call x1, Pallas kernels, local(): pl.pallas_call(functools.partial(project_kernel, tiles), grid=(3 * tiles,...  6.5 us
    unnamed x9, local copies, waits for them, and re-layouts  3.92 us
    pallas_call x1, Pallas kernels, local(): pl.pallas_call(functools.partial(mix_kernel, splits), in_specs=[in_vmem()...  2.6 us

profile of v1, /device:TPU:25, one launch (start us, length us, event | category | flops | bytes accessed | tf_op | source)
XLA Modules:
  0.0 73.3 jit_solution(5262828761790252491)
XLA Ops:
  0.6 0.0 copy-start.2
  0.7 0.9 %copy.36.chosen_ref = s32[64,16]{1,0:T(8,128)S(1)} copy(s32[64,16]{0,1:T(8,128)} %param.11) | data formatting | bytes 8192 | tf_op args[5]
  1.5 0.1 eq.28
  1.6 0.2 fusion
  1.9 0.1 copy.29
  2.0 0.1 copy.30
  2.0 0.1 multiply_reduce_fusion
  2.1 0.1 copy.33
  2.3 0.1 copy.31
  2.4 0.1 copy.37.slot_ref
  2.4 0.1 copy.34
  2.5 0.1 copy.35.sel_ref
  2.6 0.6 fusion.2
  3.1 0.3 pad_maximum_fusion
  3.4 0.0 copy-done.2
  3.4 0.0 copy-start.1
  3.4 1.6 %copy-done.1 = bf16[2048,512]{1,0:T(8,128)(2,1)S(1)} copy-done((bf16[2048,512]{1,0:T(8,128)(2,1)S(1)}, bf16[2048,512]{1,0:T(8,128)(2,1)}, u32[]{:S(2)}) %copy-start.1) | copy-done | bytes 2097176
  5.0 6.5 %project.1 = (bf16[4,256,256]{2,1,0:T(8,128)(2,1)S(1)}, bf16[256,512]{1,0:T(8,128)(2,1)S(1)}) custom-call(bf16[256,2048]{1,0:T(8,128)(2,1)S(1)} %copy-done.2, bf16[2048,512]{1,0:T(8,128)(2,1)S(1)} %copy-done.1, bf16[2048,512]{1,0:T(8,128)(2,1)} %wv_ref.1, bf16[2048,512]{1,0:T(8,128)(2,1)} %wq_ref.1, f32[256,128]{1,0:T(8,128)S(1)} %get-tuple-element.21.cos_ref, ...), custom_call_target="tpu_custom_call" | custom-call | tf_op jit(solution)/shard_map/project/pallas_call | solution.py:296
  11.5 49.4 %exchange.1.tab_ref = bf16[4,2560,256]{2,1,0:T(8,128)(2,1)S(1)} custom-call(s32[16,32]{1,0:T(8,128)S(1)} %copy.35.sel_ref, bf16[4,256,256]{2,1,0:T(8,128)(2,1)S(1)} %get-tuple-element.7.kv_ref), custom_call_target="tpu_custom_call" | custom-call | tf_op jit(solution)/shard_map/exchange/pallas_call | solution.py:331
  61.0 0.0 copy-start
  61.0 8.2 %attend.1 = (bf16[256,512]{1,0:T(8,128)(2,1)S(1)}, f32[256,128]{1,0:T(8,128)S(1)}) custom-call(s32[64,16]{1,0:T(8,128)S(1)} %copy.36.chosen_ref, s32[16,64]{1,0:T(8,128)S(1)} %copy.37.slot_ref, bf16[256,512]{1,0:T(8,128)(2,1)S(1)} %get-tuple-element.6.q_ref, bf16[4,2560,256]{2,1,0:T(8,128)(2,1)S(1)} %exchange.1.tab_ref), custom_call_target="tpu_custom_call" | custom-call | tf_op jit(solution)/shard_map/attend/pallas_call | solution.py:350
  69.2 0.7 copy.38
  69.9 2.6 %mix.1 = bf16[128,2048]{1,0:T(8,128)(2,1)S(1)} custom-call(bf16[256,512]{1,0:T(8,128)(2,1)S(1)} %get-tuple-element.8.att_ref, bf16[512,2048]{1,0:T(8,128)(2,1)S(1)} %copy-done), custom_call_target="tpu_custom_call" | custom-call | tf_op jit(solution)/shard_map/mix/pallas_call | solution.py:367
  72.5 0.8 %copy.40 = bf16[128,2048]{1,0:T(8,128)(2,1)} copy(bf16[128,2048]{1,0:T(8,128)(2,1)S(1)} %mix.1) | data formatting | bytes 1048576
  (9 shorter events, 0.1 us)
Async XLA Ops:
  0.6 2.8 %copy-start.2 = (bf16[256,2048]{1,0:T(8,128)(2,1)S(1)}, bf16[256,2048]{1,0:T(8,128)(2,1)}, u32[]{:S(2)}) copy-start(bf16[256,2048]{1,0:T(8,128)(2,1)} %x_ref.1) | copy-start | bytes 3145732
  3.4 1.6 %copy-start.1 = (bf16[2048,512]{1,0:T(8,128)(2,1)S(1)}, bf16[2048,512]{1,0:T(8,128)(2,1)}, u32[]{:S(2)}) copy-start(bf16[2048,512]{1,0:T(8,128)(2,1)} %wk_ref.1) | copy-start | bytes 6291460
  61.0 8.9 %copy-start = (bf16[512,2048]{1,0:T(8,128)(2,1)S(1)}, bf16[512,2048]{1,0:T(8,128)(2,1)}, u32[]{:S(2)}) copy-start(bf16[512,2048]{1,0:T(8,128)(2,1)} %w_ref.1) | copy-start | bytes 6291460

commit v2 on v1

v2 whole, which is shorter than its diff:
```python
import functools

import jax
import jax.numpy as jnp
from jax import lax
from jax.experimental import pallas as pl
from jax.experimental.pallas import tpu as pltpu
from jax.sharding import PartitionSpec as P

HEAD_DIM = 64
BLK = 64
CAP = 2
LANES = 128
VMEM_LIMIT = 48 * 1024 * 1024

rotary_base = 500000.0
masked_score = -1e30


def in_vmem():
    return pl.BlockSpec(memory_space=pltpu.VMEM)


def in_smem():
    return pl.BlockSpec(memory_space=pltpu.SMEM)


def attention_kernel(
    layers, group, blocks, places_ref, sel_ref, x_ref, wk_ref, wv_ref, wq_ref, cos_ref, sin_ref,
    out_ref, log_ref, wkv, wq, query, stage, picked, load_sem, col_send, col_recv, pl_send, pl_recv, *tables
):
    pairs = len(tables)
    entries = places_ref.shape[1] - 1
    me = lax.axis_index("kv")
    z = lax.div(me, group)
    g = lax.rem(me, group)
    up = lax.rem(me + group, layers * group)
    down = lax.rem(me + (layers - 1) * group, layers * group)
    half = HEAD_DIM // 2
    mesh_ids = pl.DeviceIdType.MESH
    peers = [z * group + lax.rem(g + d, group) for d in range(group)]

    def load(kind, ch):
        lanes = pl.ds(ch * LANES, LANES)
        source = (wk_ref, wv_ref, wq_ref)[kind].at[:, lanes]
        if kind < 2:
            target = wkv.at[ch, :, pl.ds(kind * LANES, LANES)]
        else:
            target = wq.at[:, lanes]
        return pltpu.make_async_copy(source, target, load_sem.at[kind, ch])

    for ch in range(pairs):
        load(0, ch).start()
        load(1, ch).start()
    for ch in range(pairs):
        load(2, ch).start()

    barrier = pltpu.get_barrier_semaphore()
    for d in range(1, group):
        pl.semaphore_signal(barrier, inc=1, device_id={"kv": peers[d]}, device_id_type=mesh_ids)

    @pl.when(z < layers - 1)
    def _():
        pl.semaphore_signal(barrier, inc=1, device_id={"kv": up}, device_id_type=mesh_ids)

    @pl.when(z > 0)
    def _():
        pl.semaphore_signal(barrier, inc=1, device_id={"kv": down}, device_id_type=mesh_ids)

    def column_copy(t, ch):
        return pltpu.make_async_remote_copy(
            src_ref=tables[ch].at[pl.ds(t * blocks, blocks)],
            dst_ref=tables[ch].at[pl.ds((t + 1) * blocks, blocks)],
            send_sem=col_send.at[t, ch],
            recv_sem=col_recv.at[t, ch],
            device_id={"kv": up},
            device_id_type=mesh_ids,
        )

    def plane_copy(d, t, ch):
        place = layers * blocks + ((d - 1) * layers + t) * CAP
        return pltpu.make_async_remote_copy(
            src_ref=stage.at[d - 1, t, ch],
            dst_ref=tables[ch].at[pl.ds(place, CAP)],
            send_sem=pl_send.at[d - 1, t, ch],
            recv_sem=pl_recv.at[d - 1, t, ch],
            device_id={"kv": peers[d]},
            device_id_type=mesh_ids,
        )

    def hand_on(d, t, ch):
        for c in range(CAP):
            index = sel_ref[peers[d], ((z - t) * group + g) * CAP + c]
            chosen_tile = None
            for i in range(blocks):
                tile = tables[ch][t * blocks + i]
                chosen_tile = tile if chosen_tile is None else jnp.where(index == i, tile, chosen_tile)
            stage[d - 1, t, ch, c] = chosen_tile
        plane_copy(d, t, ch).start()

    def send_set(t, ch):
        if t < layers - 1:

            @pl.when(z < layers - 1)
            def _():
                column_copy(t, ch).start()

        for d in range(1, group):
            if t == 0:
                pl.when(g + d < group)(functools.partial(hand_on, d, t, ch))
            else:
                hand_on(d, t, ch)

    cos_part = cos_ref[...]
    sin_part = sin_ref[...]
    low = lax.broadcasted_iota(jnp.int32, cos_part.shape, 1) % HEAD_DIM < half

    def turned(part):
        other = jnp.where(low, pltpu.roll(part, LANES - half, 1), pltpu.roll(part, half, 1))
        return part * cos_part + other * sin_part

    for ch in range(pairs):
        load(0, ch).wait()
        load(1, ch).wait()
        made = jnp.dot(x_ref[...], wkv[ch], preferred_element_type=jnp.float32)
        key_rows = turned(made[:, :LANES]).astype(jnp.bfloat16)
        value_rows = made[:, LANES:].astype(jnp.bfloat16)
        for i in range(blocks):
            tables[ch][i, :, :LANES] = key_rows[i * BLK : (i + 1) * BLK]
            tables[ch][i, :, LANES:] = value_rows[i * BLK : (i + 1) * BLK]
        if ch == 0:
            pl.semaphore_wait(barrier, group - 1 + jnp.minimum(z, 1) + jnp.minimum(layers - 1 - z, 1))
        send_set(0, ch)

    for ch in range(pairs):
        load(2, ch).wait()
    wide = min(2 * LANES, pairs * LANES)
    for lane in range(0, pairs * LANES, wide):
        made = jnp.dot(x_ref[...], wq[:, lane : lane + wide], preferred_element_type=jnp.float32)
        for part in range(0, wide, LANES):
            piece = turned(made[:, part : part + LANES]).astype(jnp.bfloat16)
            query[:, lane + part : lane + part + LANES] = (piece * (HEAD_DIM**-0.5)).astype(jnp.bfloat16)

    first = lax.broadcasted_iota(jnp.int32, (BLK, LANES), 1) < HEAD_DIM
    lane_index = lax.broadcasted_iota(jnp.int32, (BLK, LANES), 1)

    def attend(ch):
        lanes = slice(ch * LANES, (ch + 1) * LANES)

        def one_block(r, carry):
            count = places_ref[r, entries]
            for s in range(entries):
                picked[s * BLK : (s + 1) * BLK, :] = tables[ch][places_ref[r, s]]
            rows = pl.ds(pl.multiple_of(r * BLK, BLK), BLK)
            live = lax.broadcasted_iota(jnp.int32, (2 * BLK, entries * BLK), 1) < count * BLK
            both = query[rows, lanes]
            none = jnp.zeros_like(both)
            stacked = jnp.concatenate([jnp.where(first, both, none), jnp.where(first, none, both)], axis=0)
            scores = lax.dot_general(
                stacked, picked[:, :LANES], (((1,), (1,)), ((), ())), preferred_element_type=jnp.float32
            )
            scores = jnp.where(live, scores, masked_score)
            top = jnp.max(scores, axis=1, keepdims=True)
            weights = jnp.exp(scores - top)
            total = jnp.sum(weights, axis=1, keepdims=True)
            summed = jnp.dot(
                weights.astype(jnp.bfloat16), picked[:, LANES:], preferred_element_type=jnp.float32
            )
            summed = summed / total
            out_ref[rows, lanes] = jnp.where(first, summed[:BLK], summed[BLK:]).astype(jnp.bfloat16)
            log_sum = top + jnp.log(total)
            logs = jnp.zeros((BLK, LANES), jnp.float32) if ch == 0 else log_ref[rows, :]
            logs = jnp.where(lane_index == 2 * ch, log_sum[:BLK], logs)
            log_ref[rows, :] = jnp.where(lane_index == 2 * ch + 1, log_sum[BLK:], logs)
            return carry

        lax.fori_loop(0, blocks, one_block, 0)

    def finish(ch):
        for t in range(layers):

            @pl.when(z >= t)
            def _():
                for d in range(1, group):
                    if t == 0:
                        pl.when(g >= d)(lambda d=d: plane_copy(d, t, ch).wait_recv())
                    else:
                        plane_copy(d, t, ch).wait_recv()

        attend(ch)

    for ch in range(pairs):
        for t in range(1, layers):

            @pl.when(z >= t)
            def _():
                column_copy(t - 1, ch).wait_recv()
                send_set(t, ch)

        if ch > 0:
            finish(ch - 1)
    finish(pairs - 1)

    for ch in range(pairs):
        for t in range(layers):

            @pl.when(z >= t)
            def _():
                if t < layers - 1:

                    @pl.when(z < layers - 1)
                    def _():
                        column_copy(t, ch).wait_send()

                for d in range(1, group):
                    if t == 0:
                        pl.when(g + d < group)(lambda d=d: plane_copy(d, t, ch).wait_send())
                    else:
                        plane_copy(d, t, ch).wait_send()


def mix_kernel(n, att_ref, w_ref, out_ref, stage, landed, send_sem, recv_sem):
    me = lax.axis_index("tp")
    rows = out_ref.shape[0]
    tile = min(512, w_ref.shape[1])
    tiles = w_ref.shape[1] // tile
    peers = [lax.rem(me + d, n) for d in range(n)]
    barrier = pltpu.get_barrier_semaphore()
    for d in range(1, n):
        pl.semaphore_signal(barrier, inc=1, device_id={"tp": peers[d]}, device_id_type=pl.DeviceIdType.MESH)
    pl.semaphore_wait(barrier, n - 1)

    def partial_of(d, j):
        mine = att_ref[pl.ds(pl.multiple_of(peers[d] * rows, rows), rows), :]
        made = jnp.dot(mine, w_ref[:, j * tile : (j + 1) * tile], preferred_element_type=jnp.float32)
        return made.astype(jnp.bfloat16)

    def hop(d, j):
        return pltpu.make_async_remote_copy(
            src_ref=stage.at[d - 1, j],
            dst_ref=landed.at[d - 1, j],
            send_sem=send_sem.at[d - 1, j],
            recv_sem=recv_sem.at[d - 1, j],
            device_id={"tp": peers[d]},
            device_id_type=pl.DeviceIdType.MESH,
        )

    for d in range(1, n):
        for j in range(tiles):
            stage[d - 1, j] = partial_of(d, j)
            hop(d, j).start()
    for j in range(tiles):
        acc = partial_of(0, j).astype(jnp.float32)
        for d in range(1, n):
            hop(d, j).wait_recv()
            acc = acc + landed[d - 1, j].astype(jnp.float32)
        out_ref[:, j * tile : (j + 1) * tile] = acc.astype(jnp.bfloat16)
    for d in range(1, n):
        for j in range(tiles):
            hop(d, j).wait_send()


def local(devices, splits, tokens, w_query, w_key, w_value, w_out, chosen):
    rows, depth = tokens.shape
    width = w_query.shape[1]
    heads = width // HEAD_DIM
    blocks = rows // BLK
    group = 1
    while group * group < devices:
        group *= 2
    layers = devices // group
    all_blocks = chosen.shape[0]
    me = lax.axis_index("kv")

    half = HEAD_DIM // 2
    inverse = rotary_base ** (-jnp.arange(half, dtype=jnp.float32) / half)
    positions = (me * rows + jnp.arange(rows)).astype(jnp.float32)
    angles = positions[:, None] * inverse[None, :]
    cos_half, sin_half = jnp.cos(angles), jnp.sin(angles)
    cos_part = jnp.concatenate([cos_half] * (LANES // half), axis=1)
    sin_part = jnp.concatenate([-sin_half, sin_half] * (LANES // HEAD_DIM), axis=1)

    flat = chosen.reshape(devices, -1)
    listed = jnp.any(flat[:, :, None] == jnp.arange(all_blocks)[None, None, :], axis=1)
    listed = listed.reshape(devices, devices, blocks).astype(jnp.int32)
    before = (jnp.arange(blocks)[:, None] < jnp.arange(blocks)[None, :]).astype(jnp.int32)
    slots = jnp.sum(listed[:, :, :, None] * before[None, None], axis=2)
    fits = (slots[:, :, None, :] == jnp.arange(CAP)[:, None]) & (listed[:, :, None, :] > 0)
    sel = jnp.sum(jnp.where(fits, jnp.arange(blocks), 0), axis=-1).reshape(devices, devices * CAP)

    own_lists = lax.dynamic_slice_in_dim(chosen, me * blocks, blocks, 0)
    own_slots = lax.dynamic_slice_in_dim(slots.reshape(devices, all_blocks), me, 1, 0)
    own_blocks = jnp.where(own_lists >= 0, own_lists, me * blocks + jnp.arange(blocks)[:, None])
    every_block = jnp.arange(all_blocks)
    owners = every_block // blocks
    steps = me // group - owners // group
    across = (me % group - owners % group + group) % group
    handed = layers * blocks + ((across - 1) * layers + steps) * CAP + jnp.minimum(own_slots[0], CAP - 1)
    home = jnp.where(across == 0, steps * blocks + every_block % blocks, handed)
    places = jnp.sum(jnp.where(own_blocks[:, :, None] == every_block, home, 0), axis=-1)
    counts = jnp.sum((own_lists >= 0).astype(jnp.int32), axis=1, keepdims=True)
    places = jnp.concatenate([places, counts], axis=1)

    table_blocks = layers * blocks + (group - 1) * layers * CAP
    pairs = width // LANES
    in_hbm = pl.BlockSpec(memory_space=pltpu.HBM)
    attended, logs = pl.pallas_call(
        functools.partial(attention_kernel, layers, group, blocks),
        in_specs=[in_smem()] * 2 + [in_vmem()] + [in_hbm] * 3 + [in_vmem()] * 2,
        out_specs=[in_vmem(), in_vmem()],
        out_shape=[
            jax.ShapeDtypeStruct((rows, width), jnp.bfloat16),
            jax.ShapeDtypeStruct((rows, LANES), jnp.float32),
        ],
        scratch_shapes=[
            pltpu.VMEM((pairs, depth, 2 * LANES), jnp.bfloat16),
            pltpu.VMEM((depth, width), jnp.bfloat16),
            pltpu.VMEM((rows, width), jnp.bfloat16),
            pltpu.VMEM((group - 1, layers, pairs, CAP, BLK, 2 * LANES), jnp.bfloat16),
            pltpu.VMEM((chosen.shape[1] * BLK, 2 * LANES), jnp.bfloat16),
            pltpu.SemaphoreType.DMA((3, pairs)),
            pltpu.SemaphoreType.DMA((layers, pairs)),
            pltpu.SemaphoreType.DMA((layers, pairs)),
            pltpu.SemaphoreType.DMA((group - 1, layers, pairs)),
            pltpu.SemaphoreType.DMA((group - 1, layers, pairs)),
        ]
        + [pltpu.VMEM((table_blocks, BLK, 2 * LANES), jnp.bfloat16)] * pairs,
        compiler_params=pltpu.CompilerParams(
            collective_id=0, has_side_effects=True, vmem_limit_bytes=VMEM_LIMIT
        ),
        name="attention",
    )(places, sel, tokens, w_key, w_value, w_query, cos_part, sin_part)
    log_sums = jnp.transpose(logs[:, :heads])

    out_rows = rows // splits
    tile = min(512, w_out.shape[1])
    out_tiles = w_out.shape[1] // tile
    output = pl.pallas_call(
        functools.partial(mix_kernel, splits),
        in_specs=[in_vmem(), in_vmem()],
        out_specs=in_vmem(),
        out_shape=jax.ShapeDtypeStruct((out_rows, w_out.shape[1]), jnp.bfloat16),
        scratch_shapes=[
            pltpu.VMEM((splits - 1, out_tiles, out_rows, tile), jnp.bfloat16),
            pltpu.VMEM((splits - 1, out_tiles, out_rows, tile), jnp.bfloat16),
            pltpu.SemaphoreType.DMA((splits - 1, out_tiles)),
            pltpu.SemaphoreType.DMA((splits - 1, out_tiles)),
        ],
        compiler_params=pltpu.CompilerParams(
            collective_id=1, has_side_effects=True, vmem_limit_bytes=VMEM_LIMIT
        ),
        name="mix",
    )(attended, w_out)
    return (output, log_sums)


def solution(mesh):
    placed = (P("kv", None), P(None, "tp"), P(None, "tp"), P(None, "tp"), P("tp", None), P())
    return jax.shard_map(
        functools.partial(local, mesh.shape["kv"], mesh.shape["tp"]),
        mesh=mesh,
        in_specs=placed,
        out_specs=(P(("kv", "tp"), None), P("tp", "kv")),
        check_vma=False,
    )
```

time: 74.5 us -> 66.8 us (0.90); the launches traced: 73.3 us -> 66.5 us
  Pallas kernels: 66.8 us -> 57 us
  local copies, waits for them, and re-layouts: 4.55 us -> 6.17 us
  other arithmetic: 1.21 us -> 2.56 us
    pallas_call x3 -> x1, Pallas kernels: 64.2 us -> 50.2 us  [local(): pl.pallas_call(functools.partial(attention_kernel, layers, group, blocks)...]
    pallas_call x1, Pallas kernels: 2.6 us -> 6.83 us  [local(): pl.pallas_call(functools.partial(mix_kernel, splits), in_specs=[in_vmem()...]
    unnamed x9 -> x11, local copies, waits for them, and re-layouts: 3.92 us -> 5.43 us
    select_n x0 -> x2, other arithmetic: none -> 0.89 us  [the longest x1 0.86 us: local(): jnp.where(own_lists >= 0, own_lists, me * blocks + jnp.arange(blocks)[:,...]
where the time goes in v2:
time: 66.8 us; the launch traced here: 66.5 us
  Pallas kernels  57 us (85%)
  local copies, waits for them, and re-layouts  6.17 us (9%)
  other arithmetic  2.56 us (4%)
  between operations  0.78 us (1%)
    pallas_call x1, Pallas kernels, local(): pl.pallas_call(functools.partial(attention_kernel, layers, group, blocks)...  50.2 us
    pallas_call x1, Pallas kernels, local(): pl.pallas_call(functools.partial(mix_kernel, splits), in_specs=[in_vmem()...  6.83 us
    unnamed x11, local copies, waits for them, and re-layouts  5.43 us

profile of v2, /device:TPU:25, one launch (start us, length us, event | category | flops | bytes accessed | tf_op | source)
XLA Modules:
  0.0 66.5 jit_solution(11029460809448338800)
XLA Ops:
  0.7 0.9 %compare_select_fusion = (s32[4,16]{0,1:T(8,128)S(1)}, s32[4]{0:T(128)S(1)}) fusion(s32[64,16]{0,1:T(8,128)} %param.11, s32[]{:T(128)S(6)} %select_n.56, s32[4]{0:T(128)S(1)} %iota_add_fusion), kind=kLoop, calls=%fused_computation.17 | loop fusion | flops 252 | bytes 548 | tf_op jit(solution)/shard_map/jit(_where)/select_n | solution.py:293
  1.6 0.1 copy.37
  1.7 0.1 copy.42
  1.7 0.8 %copy.38 = s32[64,16]{1,0:T(8,128)S(1)} copy(s32[64,16]{0,1:T(8,128)} %param.11) | data formatting | bytes 8192 | tf_op args[5]
  2.5 0.1 eq.55
  2.6 0.2 fusion
  2.8 0.1 copy.39
  3.0 0.1 copy.40
  3.0 0.1 multiply_reduce_fusion
  3.1 0.1 copy.43
  3.2 0.1 copy.41
  3.3 0.2 minimum_reduce_fusion
  3.5 0.2 select_reduce_fusion.1
  3.8 0.1 pad_add_fusion.places_ref
  3.8 0.1 copy.44
  3.9 0.1 copy.46.sel_ref
  4.0 0.5 fusion.2
  4.5 0.3 pad_maximum_fusion
  4.8 1.6 %copy-done = bf16[2048,512]{1,0:T(8,128)(2,1)S(1)} copy-done((bf16[2048,512]{1,0:T(8,128)(2,1)S(1)}, bf16[2048,512]{1,0:T(8,128)(2,1)}, u32[]{:S(2)}) %copy-start) | copy-done | bytes 2097176
  6.4 1.6 %copy-done.1 = bf16[2048,512]{1,0:T(8,128)(2,1)S(1)} copy-done((bf16[2048,512]{1,0:T(8,128)(2,1)S(1)}, bf16[2048,512]{1,0:T(8,128)(2,1)}, u32[]{:S(2)}) %copy-start.1) | copy-done | bytes 2097176
  8.0 50.2 %attention.1 = (bf16[256,512]{1,0:T(8,128)(2,1)S(1)}, f32[256,128]{1,0:T(8,128)S(1)}) custom-call(s32[4,17]{1,0:T(4,128)S(1)} %pad_add_fusion.places_ref, s32[16,32]{1,0:T(8,128)S(1)} %copy.46.sel_ref, bf16[256,2048]{1,0:T(8,128)(2,1)S(1)} %copy-done.3, bf16[2048,512]{1,0:T(8,128)(2,1)S(1)} %copy-done, bf16[2048,512]{1,0:T(8,128)(2,1)S(1)} %copy-done.1, ...), custom_call_target="tpu_custom_call" | custom-call | tf_op jit(solution)/shard_map/attention/pallas_call | solution.py:307
  58.2 0.7 %copy.47 = f32[8,256]{1,0:T(8,128)} copy(f32[8,256]{0,1:T(8,128)S(1)} %slice_bitcast_fusion) | data formatting | bytes 16384
  58.9 6.8 %mix.1 = bf16[128,2048]{1,0:T(8,128)(2,1)S(1)} custom-call(bf16[256,512]{1,0:T(8,128)(2,1)S(1)} %get-tuple-element.4.att_ref, bf16[512,2048]{1,0:T(8,128)(2,1)S(1)} %copy-done.2), custom_call_target="tpu_custom_call" | custom-call | tf_op jit(solution)/shard_map/mix/pallas_call | solution.py:338
  65.7 0.8 %copy.49 = bf16[128,2048]{1,0:T(8,128)(2,1)} copy(bf16[128,2048]{1,0:T(8,128)(2,1)S(1)} %mix.1) | data formatting | bytes 1048576
  (15 shorter events, 0.1 us)
Async XLA Ops:
  0.6 4.2 %copy-start.3 = (bf16[256,2048]{1,0:T(8,128)(2,1)S(1)}, bf16[256,2048]{1,0:T(8,128)(2,1)}, u32[]{:S(2)}) copy-start(bf16[256,2048]{1,0:T(8,128)(2,1)} %x_ref.1) | copy-start | bytes 3145732
  4.8 1.6 %copy-start = (bf16[2048,512]{1,0:T(8,128)(2,1)S(1)}, bf16[2048,512]{1,0:T(8,128)(2,1)}, u32[]{:S(2)}) copy-start(bf16[2048,512]{1,0:T(8,128)(2,1)} %wk_ref.1) | copy-start | bytes 6291460
  6.4 1.6 %copy-start.1 = (bf16[2048,512]{1,0:T(8,128)(2,1)S(1)}, bf16[2048,512]{1,0:T(8,128)(2,1)}, u32[]{:S(2)}) copy-start(bf16[2048,512]{1,0:T(8,128)(2,1)} %wv_ref.1) | copy-start | bytes 6291460
  8.0 50.9 %copy-start.2 = (bf16[512,2048]{1,0:T(8,128)(2,1)S(1)}, bf16[512,2048]{1,0:T(8,128)(2,1)}, u32[]{:S(2)}) copy-start(bf16[512,2048]{1,0:T(8,128)(2,1)} %w_ref.1) | copy-start | bytes 6291460

commit v3 on v2

--- a/solution.py
+++ b/solution.py
@@ -11,7 +11,7 @@
 BLK = 64
 CAP = 2
 LANES = 128
-VMEM_LIMIT = 48 * 1024 * 1024
+VMEM_LIMIT = 62 * 1024 * 1024
 
 rotary_base = 500000.0
 masked_score = -1e30
@@ -26,8 +26,8 @@
 
 
 def attention_kernel(
-    layers, group, blocks, places_ref, sel_ref, x_ref, wk_ref, wv_ref, wq_ref, cos_ref, sin_ref,
-    out_ref, log_ref, wkv, wq, query, stage, picked, load_sem, col_send, col_recv, pl_send, pl_recv, *tables
+    layers, group, blocks, splits, places_ref, sel_ref, tokens_ref, wk_ref, wv_ref, wq_ref, wo_ref, cos_ref, sin_ref,
+    mixed_ref, log_ref, x_ref, wo, out_ref, part_stage, landed, part_send, part_recv, side_sem, wkv, wq, query, stage, picked, load_sem, col_send, col_recv, pl_send, pl_recv, *tables
 ):
     pairs = len(tables)
     entries = places_ref.shape[1] - 1
@@ -49,13 +49,21 @@
             target = wq.at[:, lanes]
         return pltpu.make_async_copy(source, target, load_sem.at[kind, ch])
 
+    token_load = pltpu.make_async_copy(tokens_ref, x_ref, side_sem.at[0])
+    out_load = pltpu.make_async_copy(wo_ref, wo, side_sem.at[1])
+    token_load.start()
     for ch in range(pairs):
         load(0, ch).start()
         load(1, ch).start()
     for ch in range(pairs):
         load(2, ch).start()
+    out_load.start()
 
     barrier = pltpu.get_barrier_semaphore()
+    side = lax.axis_index("tp")
+    others = [lax.rem(side + d, splits) for d in range(splits)]
+    for d in range(1, splits):
+        pl.semaphore_signal(barrier, inc=1, device_id={"tp": others[d]}, device_id_type=mesh_ids)
     for d in range(1, group):
         pl.semaphore_signal(barrier, inc=1, device_id={"kv": peers[d]}, device_id_type=mesh_ids)
 
@@ -119,6 +127,7 @@
         other = jnp.where(low, pltpu.roll(part, LANES - half, 1), pltpu.roll(part, half, 1))
         return part * cos_part + other * sin_part
 
+    token_load.wait()
     for ch in range(pairs):
         load(0, ch).wait()
         load(1, ch).wait()
@@ -129,7 +138,7 @@
             tables[ch][i, :, :LANES] = key_rows[i * BLK : (i + 1) * BLK]
             tables[ch][i, :, LANES:] = value_rows[i * BLK : (i + 1) * BLK]
         if ch == 0:
-            pl.semaphore_wait(barrier, group - 1 + jnp.minimum(z, 1) + jnp.minimum(layers - 1 - z, 1))
+            pl.semaphore_wait(barrier, splits + group - 2 + jnp.minimum(z, 1) + jnp.minimum(layers - 1 - z, 1))
         send_set(0, ch)
 
     for ch in range(pairs):
@@ -218,44 +227,37 @@
                     else:
                         plane_copy(d, t, ch).wait_send()
 
-
-def mix_kernel(n, att_ref, w_ref, out_ref, stage, landed, send_sem, recv_sem):
-    me = lax.axis_index("tp")
-    rows = out_ref.shape[0]
-    tile = min(512, w_ref.shape[1])
-    tiles = w_ref.shape[1] // tile
-    peers = [lax.rem(me + d, n) for d in range(n)]
-    barrier = pltpu.get_barrier_semaphore()
-    for d in range(1, n):
-        pl.semaphore_signal(barrier, inc=1, device_id={"tp": peers[d]}, device_id_type=pl.DeviceIdType.MESH)
-    pl.semaphore_wait(barrier, n - 1)
+    rows_out = mixed_ref.shape[0]
+    tile = min(512, wo.shape[1])
+    tiles = wo.shape[1] // tile
+    out_load.wait()
 
     def partial_of(d, j):
-        mine = att_ref[pl.ds(pl.multiple_of(peers[d] * rows, rows), rows), :]
-        made = jnp.dot(mine, w_ref[:, j * tile : (j + 1) * tile], preferred_element_type=jnp.float32)
+        mine = out_ref[pl.ds(pl.multiple_of(others[d] * rows_out, rows_out), rows_out), :]
+        made = jnp.dot(mine, wo[:, j * tile : (j + 1) * tile], preferred_element_type=jnp.float32)
         return made.astype(jnp.bfloat16)
 
     def hop(d, j):
         return pltpu.make_async_remote_copy(
-            src_ref=stage.at[d - 1, j],
+            src_ref=part_stage.at[d - 1, j],
             dst_ref=landed.at[d - 1, j],
-            send_sem=send_sem.at[d - 1, j],
-            recv_sem=recv_sem.at[d - 1, j],
-            device_id={"tp": peers[d]},
-            device_id_type=pl.DeviceIdType.MESH,
+            send_sem=part_send.at[d - 1, j],
+            recv_sem=part_recv.at[d - 1, j],
+            device_id={"tp": others[d]},
+            device_id_type=mesh_ids,
         )
 
-    for d in range(1, n):
+    for d in range(1, splits):
         for j in range(tiles):
-            stage[d - 1, j] = partial_of(d, j)
+            part_stage[d - 1, j] = partial_of(d, j)
             hop(d, j).start()
     for j in range(tiles):
         acc = partial_of(0, j).astype(jnp.float32)
-        for d in range(1, n):
+        for d in range(1, splits):
             hop(d, j).wait_recv()
             acc = acc + landed[d - 1, j].astype(jnp.float32)
-        out_ref[:, j * tile : (j + 1) * tile] = acc.astype(jnp.bfloat16)
-    for d in range(1, n):
+        mixed_ref[:, j * tile : (j + 1) * tile] = acc.astype(jnp.bfloat16)
+    for d in range(1, splits):
         for j in range(tiles):
             hop(d, j).wait_send()
 
@@ -304,15 +306,27 @@
     table_blocks = layers * blocks + (group - 1) * layers * CAP
     pairs = width // LANES
     in_hbm = pl.BlockSpec(memory_space=pltpu.HBM)
-    attended, logs = pl.pallas_call(
-        functools.partial(attention_kernel, layers, group, blocks),
-        in_specs=[in_smem()] * 2 + [in_vmem()] + [in_hbm] * 3 + [in_vmem()] * 2,
+    out_width = w_out.shape[1]
+    out_rows = rows // splits
+    tile = min(512, out_width)
+    parts = (splits - 1, out_width // tile)
+    output, logs = pl.pallas_call(
+        functools.partial(attention_kernel, layers, group, blocks, splits),
+        in_specs=[in_smem()] * 2 + [in_hbm] * 5 + [in_vmem()] * 2,
         out_specs=[in_vmem(), in_vmem()],
         out_shape=[
-            jax.ShapeDtypeStruct((rows, width), jnp.bfloat16),
+            jax.ShapeDtypeStruct((out_rows, out_width), jnp.bfloat16),
             jax.ShapeDtypeStruct((rows, LANES), jnp.float32),
         ],
         scratch_shapes=[
+            pltpu.VMEM((rows, depth), jnp.bfloat16),
+            pltpu.VMEM((width, out_width), jnp.bfloat16),
+            pltpu.VMEM((rows, width), jnp.bfloat16),
+            pltpu.VMEM(parts + (out_rows, tile), jnp.bfloat16),
+            pltpu.VMEM(parts + (out_rows, tile), jnp.bfloat16),
+            pltpu.SemaphoreType.DMA(parts),
+            pltpu.SemaphoreType.DMA(parts),
+            pltpu.SemaphoreType.DMA((2,)),
             pltpu.VMEM((pairs, depth, 2 * LANES), jnp.bfloat16),
             pltpu.VMEM((depth, width), jnp.bfloat16),
             pltpu.VMEM((rows, width), jnp.bfloat16),
@@ -329,28 +343,9 @@
             collective_id=0, has_side_effects=True, vmem_limit_bytes=VMEM_LIMIT
         ),
         name="attention",
-    )(places, sel, tokens, w_key, w_value, w_query, cos_part, sin_part)
+    )(places, sel, tokens, w_key, w_value, w_query, w_out, cos_part, sin_part)
     log_sums = jnp.transpose(logs[:, :heads])
 
-    out_rows = rows // splits
-    tile = min(512, w_out.shape[1])
-    out_tiles = w_out.shape[1] // tile
-    output = pl.pallas_call(
-        functools.partial(mix_kernel, splits),
-        in_specs=[in_vmem(), in_vmem()],
-        out_specs=in_vmem(),
-        out_shape=jax.ShapeDtypeStruct((out_rows, w_out.shape[1]), jnp.bfloat16),
-        scratch_shapes=[
-            pltpu.VMEM((splits - 1, out_tiles, out_rows, tile), jnp.bfloat16),
-            pltpu.VMEM((splits - 1, out_tiles, out_rows, tile), jnp.bfloat16),
-            pltpu.SemaphoreType.DMA((splits - 1, out_tiles)),
-            pltpu.SemaphoreType.DMA((splits - 1, out_tiles)),
-        ],
-        compiler_params=pltpu.CompilerParams(
-            collective_id=1, has_side_effects=True, vmem_limit_bytes=VMEM_LIMIT
-        ),
-        name="mix",
-    )(attended, w_out)
     return (output, log_sums)
 
 

time: 66.8 us -> 70.1 us (1.049)
  Pallas kernels: 57 us -> 59.7 us
  other arithmetic: 2.56 us -> 3.77 us
    pallas_call x2 -> x1, Pallas kernels: 57 us -> 59.7 us  [local(): pl.pallas_call(functools.partial(attention_kernel, layers, group, blocks,...]
    unnamed x11 -> x3, local copies, waits for them, and re-layouts: 5.43 us -> 3.33 us
    transpose x1, local copies, waits for them, and re-layouts: 0.01 us -> 0.91 us  [local(): log_sums = jnp.transpose(logs[:, :heads])]
where the time goes in v3:
time: 70.1 us; the launch traced here: 69.8 us
  Pallas kernels  59.7 us (85%)
  local copies, waits for them, and re-layouts  5.57 us (8%)
  other arithmetic  3.77 us (5%)
  between operations  0.74 us (1%)
    pallas_call x1, Pallas kernels, local(): pl.pallas_call(functools.partial(attention_kernel, layers, group, blocks,...  59.7 us
    unnamed x3, local copies, waits for them, and re-layouts  3.33 us

profile of v3, /device:TPU:25, one launch (start us, length us, event | category | flops | bytes accessed | tf_op | source)
XLA Modules:
  0.0 69.8 jit_solution(1580941586973600030)
XLA Ops:
  0.7 0.8 %compare_select_fusion = (s32[4,16]{0,1:T(8,128)S(1)}, s32[4]{0:T(128)S(1)}) fusion(s32[64,16]{0,1:T(8,128)} %param.11, s32[]{:T(128)S(6)} %select_n.56, s32[4]{0:T(128)S(1)} %iota_add_fusion), kind=kLoop, calls=%fused_computation.17 | loop fusion | flops 252 | bytes 548 | tf_op jit(solution)/shard_map/jit(_where)/select_n | solution.py:295
  1.5 0.1 copy.37
  1.6 0.1 copy.42
  1.7 0.8 %copy.38 = s32[64,16]{1,0:T(8,128)S(1)} copy(s32[64,16]{0,1:T(8,128)} %param.11) | data formatting | bytes 8192 | tf_op args[5]
  2.4 0.1 eq.55
  2.5 0.2 fusion
  2.8 0.1 copy.39
  2.9 0.1 copy.40
  2.9 0.1 multiply_reduce_fusion
  3.0 0.1 copy.43
  3.2 0.1 copy.41
  3.2 0.2 minimum_reduce_fusion
  3.5 0.2 select_reduce_fusion.1
  3.7 0.7 pad_add_fusion.places_ref
  4.3 0.1 copy.44
  4.4 0.7 copy.46.sel_ref
  5.1 0.5 fusion.2
  5.6 1.0 %pad_maximum_fusion = (f32[256,128]{1,0:T(8,128)}, f32[256,128]{1,0:T(8,128)}) fusion(f32[256,32]{1,0:T(8,128)S(1)} %get-tuple-element.20, f32[256,32]{1,0:T(8,128)S(1)} %get-tuple-element.19, f32[256,32]{1,0:T(8,128)S(1)} %get-tuple-element.18), kind=kLoop, calls=%fused_computation.4 | loop fusion | flops 196608 | bytes 360448 | tf_op jit(solution)/shard_map/concatenate | solution.py:282
  6.6 59.7 %attention.1 = (bf16[128,2048]{1,0:T(8,128)(2,1)}, f32[256,128]{1,0:T(8,128)}) custom-call(s32[4,17]{1,0:T(4,128)} %pad_add_fusion.places_ref, s32[16,32]{1,0:T(8,128)} %copy.46.sel_ref, bf16[256,2048]{1,0:T(8,128)(2,1)} %tokens_ref.1, bf16[2048,512]{1,0:T(8,128)(2,1)} %wk_ref.1, bf16[2048,512]{1,0:T(8,128)(2,1)} %wv_ref.1, bf16[2048,512]{1,0:T(8,128)(2,1)} %wq_ref.1, ...), custom_call_target="tpu_custom_call" | custom-call | tf_op jit(solution)/shard_map/attention/pallas_call | solution.py:313
  66.3 0.9 %slice_bitcast_fusion = f32[8,256]{0,1:T(8,128)S(1)} fusion(f32[256,128]{1,0:T(8,128)} %get-tuple-element.5), kind=kLoop, calls=%fused_computation.6 | loop fusion | bytes 16384 | tf_op jit(solution)/shard_map/transpose | solution.py:347
  67.2 0.7 copy.47
  67.9 1.9 %copy.49 = bf16[128,2048]{1,0:T(8,128)(2,1)} copy(bf16[128,2048]{1,0:T(8,128)(2,1)} %get-tuple-element.25) | data formatting | bytes 1048576
  (8 shorter events, 0.1 us)
